TPU v7x, 32 devices: a whole 2x2x4 slice. The times are simulated.
32 devices in a mesh: ep: 4 (over y, x), tp: 8 (over z, core).
Axes of the slice: x: 2, y: 2, z: 4, core: 2. Of those that a mesh axis runs over, the one named last changes fastest.
Arguments:
- tokens: bfloat16 [128, 2048], P('ep'), may hold values from -6 to 6
- norm_gain: float32 [2048], replicated, may hold values from 0.1 to 1.9
- routes: int32 [128, 2], P('ep'), may hold values from 0 to 3, all different within a row; in each aligned block of 32 rows (0 to 31, 32 to 63, ...) at most 16 rows name the same one
- gate_weights: float32 [128, 2], P('ep'), may hold values from 0.1 to 1
- expert_gate: bfloat16 [4, 2048, 8192], P('ep', None, 'tp'), may hold values from -0.125 to 0.125
- expert_up: bfloat16 [4, 2048, 8192], P('ep', None, 'tp'), may hold values from -0.125 to 0.125
- expert_down: bfloat16 [4, 8192, 2048], P('ep', 'tp'), may hold values from -0.0625 to 0.0625
Outputs:
- mixed: bfloat16 [128, 2048], P('ep', 'tp')
Inputs may be any that keep to these rules, and one draw needn't show every extreme that they name: `routes`: each row names 2 different experts; among the rows of one index of ep no expert is named by more than 16 rows.
All inputs are finite; a program needn't handle non-finite values.
Results may differ from a plain program's by a relative error of at most 0.0095.
Values may be sent and summed in bfloat16 or wider, within the bound.
A program may use at most 64 MiB of HBM per device.

v0:
```python
import jax
import jax.numpy as jnp
from jax import lax
from jax.sharding import PartitionSpec as P


def expert_rows(rows, w_gate, w_up):
    gate = jnp.dot(rows, w_gate, preferred_element_type=jnp.float32)
    upper = jnp.dot(rows, w_up, preferred_element_type=jnp.float32)
    return (jax.nn.silu(gate) * upper).astype(jnp.bfloat16)


def shards(tokens, norm_gain, routes, gate_weights, expert_gate, expert_up, expert_down):
    tok_rows, width = tokens.shape
    n_ep = lax.axis_size("ep")
    n_tp = lax.axis_size("tp")
    part_width = width // n_tp
    values = tokens.astype(jnp.float32)
    scale = lax.rsqrt(jnp.mean(values * values, axis=-1, keepdims=True) + 1e-06)
    normed = (values * scale * norm_gain[None, :]).astype(jnp.bfloat16)
    w_gate = expert_gate[0]
    w_up = expert_up[0]
    w_down = expert_down[0]
    capacity = tok_rows // 2
    picks = routes.reshape(-1)
    chosen = (picks[:, None] == jnp.arange(n_ep, dtype=jnp.int32)[None, :]).astype(jnp.int32)
    ranks = jnp.cumsum(chosen, axis=0) - chosen
    place = picks * capacity + jnp.sum(ranks * chosen, axis=1)
    table = (place[None, :] == jnp.arange(n_ep * capacity, dtype=jnp.int32)[:, None]).astype(
        jnp.float32
    )
    slots = jnp.sum(table.reshape(n_ep * capacity, tok_rows, 2), axis=2)
    buffer = jnp.dot(slots.astype(jnp.bfloat16), normed, preferred_element_type=jnp.float32)
    buffer = buffer.astype(jnp.bfloat16).reshape(n_ep, capacity, width)
    combine = jnp.sum(
        (table * gate_weights.reshape(-1)[None, :]).reshape(n_ep * capacity, tok_rows, 2), axis=2
    ).T
    received = lax.all_to_all(buffer, "ep", split_axis=0, concat_axis=0, tiled=True)
    sources = received.shape[0]
    count = received.shape[1]
    hidden = expert_rows(received.reshape(sources * count, width), w_gate, w_up)
    partial_value = jnp.dot(hidden, w_down, preferred_element_type=jnp.float32)
    outputs = lax.psum_scatter(
        partial_value.reshape(sources, count, width), "tp", scatter_dimension=2, tiled=True
    )
    back = lax.all_to_all(outputs, "ep", split_axis=0, concat_axis=0, tiled=True)
    mixed = jnp.dot(
        combine,
        back.reshape(n_ep * capacity, part_width),
        precision=lax.Precision.HIGHEST,
        preferred_element_type=jnp.float32,
    )
    return mixed.astype(jnp.bfloat16)


def solution(mesh):
    placed = (
        P("ep", None),
        P(),
        P("ep", None),
        P("ep", None),
        P("ep", None, "tp"),
        P("ep", None, "tp"),
        P("ep", "tp", None),
    )
    return jax.shard_map(
        shards, mesh=mesh, in_specs=placed, out_specs=P("ep", "tp"), check_vma=False
    )
```

profile of v0, /device:TPU:0, one launch (start us, length us, event | category | flops | bytes accessed | tf_op | source)
XLA Modules:
  0.0 75.7 jit_solution(16536749545216895119)
XLA Ops:
  6.5 0.0 reduce-scatter.2.cloned.1.call-start
  6.5 1.0 %fusion.12 = f32[32]{0:T(128)S(1)} fusion(bf16[32,2048]{1,0:T(8,128)(2,1)} %param.7), kind=kLoop, calls=%fused_computation.12 | loop fusion | flops 196576 | bytes 131200 | tf_op jit(solution)/shard_map/reduce_sum | solution.py:19
  7.6 0.8 %copy.20 = s32[32,2]{1,0:T(8,128)S(1)} copy(s32[32,2]{0,1:T(2,128)} %param.9) | data formatting | bytes 512 | tf_op args[2]
  8.4 0.1 eq.30
  8.5 0.1 fusion.18
  8.5 0.1 reduce_window_sum.11
  8.6 0.2 select_reduce_fusion.1
  8.8 0.1 reduce_sum.39
  8.9 0.1 copy.21
  9.0 0.0 copy-start.1
  9.0 0.8 %multiply_add_fusion = s32[32,2]{0,1:T(2,128)S(1)} fusion(s32[32,2]{0,1:T(2,128)S(1)} %copy.21, s32[32,2]{0,1:T(2,128)} %param.9), kind=kLoop, calls=%fused_computation.24 | loop fusion | flops 128 | bytes 768 | tf_op jit(solution)/shard_map/add | solution.py:28
  9.9 0.9 %convert_reduce_fusion = (bf16[64,32]{0,1:T(8,128)(2,1)S(1)}, f32[64,32]{0,1:T(8,128)S(1)}) fusion(s32[32,2]{0,1:T(2,128)S(1)} %multiply_add_fusion, f32[32,2]{0,1:T(2,128)} %param.10), kind=kLoop, calls=%fused_computation.17 | loop fusion | flops 16384 | bytes 12800 | tf_op jit(solution)/shard_map/reduce_sum | solution.py:32
  10.8 1.2 %convolution_convert_fusion = bf16[64,2048]{1,0:T(8,128)(2,1)S(1)} fusion(bf16[32,2048]{1,0:T(8,128)(2,1)} %param.7, f32[2048]{0:T(1024)} %param.8, f32[32]{0:T(128)S(1)} %add_rsqrt_fusion, bf16[64,32]{0,1:T(8,128)(2,1)S(1)} %get-tuple-element.5), kind=kOutput, calls=%fused_computation.6 | convolution fusion | flops 8781824 | bytes 405632 | tf_op jit(solution)/shard_map/dot_general | solution.py:33
  12.0 10.7 %all_to_all.10 = bf16[4,16,2048]{2,1,0:T(8,128)(2,1)S(1)} all-to-all(bf16[4,16,2048]{2,1,0:T(8,128)(2,1)S(1)} %bitcast.26), channel_id=1, replica_groups=mesh['ep'=4,'tp'=8] {'ep'}, dimensions={0} | all-to-all | bytes 524288 | tf_op jit(solution)/shard_map/all_to_all | solution.py:38
  22.7 0.0 copy-start
  22.7 3.2 %fusion.4 = f32[64,1024]{1,0:T(8,128)S(1)} fusion(bf16[64,2048]{1,0:T(8,128)(2,1)S(1)} %bitcast.24, bf16[1,2048,1024]{2,1,0:T(8,128)(2,1)} %param.11), kind=kOutput, calls=%fused_computation.4 | convolution fusion | flops 268435456 | bytes 4718592 | tf_op jit(solution)/shard_map/dot_general | solution.py:8
  25.9 0.0 copy-done.1
  25.9 0.8 %fusion.9 = bf16[64,1024]{1,0:T(8,128)(2,1)S(1)} fusion(bf16[64,2048]{1,0:T(8,128)(2,1)S(1)} %bitcast.25, bf16[1,2048,1024]{2,1,0:T(8,128)(2,1)S(1)} %copy-done.1, f32[64,1024]{1,0:T(8,128)S(1)} %fusion.4), kind=kOutput, calls=%fused_computation.8 | convolution fusion | flops 268828672 | bytes 4849664 | tf_op jit(solution)/shard_map/dot_general | solution.py:9
  26.8 0.0 copy-done
  26.8 1.6 %fusion = f32[4,16,2048]{2,1,0:T(8,128)} fusion(bf16[4,16,1024]{2,1,0:T(8,128)(2,1)S(1)} %bitcast.27, bf16[1,1024,2048]{2,1,0:T(8,128)(2,1)S(1)} %copy-done), kind=kOutput, calls=%fused_computation | convolution fusion | flops 268435456 | bytes 4849664 | tf_op jit(solution)/shard_map/dot_general | solution.py:42
  28.4 0.0 reduce-scatter.2.cloned.1.call-update
  28.4 31.1 %reduce-scatter.2.cloned.1.call-done = f32[4,16,256]{2,1,0:T(8,128)} async-done(((f32[4,16,2048]{2,1,0:T(8,128)}), f32[4,16,256]{2,1,0:T(8,128)}) %reduce-scatter.2.cloned.1.call-update) | async-done | bytes 65552 | tf_op jit(solution)/shard_map/reduce_scatter | solution.py:43
  59.5 8.6 %all_to_all.11 = f32[4,16,256]{2,1,0:T(8,128)S(1)} all-to-all(f32[4,16,256]{2,1,0:T(8,128)} %reduce-scatter.2.cloned.1.call-done), channel_id=1, replica_groups=mesh['ep'=4,'tp'=8] {'ep'}, dimensions={0} | all-to-all | bytes 131072 | tf_op jit(solution)/shard_map/all_to_all | solution.py:46
  68.1 0.8 %convolution_convert_fusion.1 = bf16[32,256]{1,0:T(8,128)(2,1)} fusion(f32[64,32]{0,1:T(8,128)S(1)} %get-tuple-element.6, f32[64,256]{1,0:T(8,128)S(1)} %bitcast.28), kind=kOutput, calls=%fused_computation.9 | convolution fusion | flops 6299648 | bytes 90112 | tf_op jit(solution)/shard_map/dot_general | solution.py:47
  (1 shorter events, 0.0 us)
Async XLA Ops:
  6.5 53.0 %reduce-scatter.2.cloned.1.call-start = ((), (), s32[]{:S(2)}) async-start(), calls=%async_computation.3 | async-start | bytes 589824 | tf_op jit(solution)/shard_map/reduce_scatter | solution.py:43
  9.0 16.9 %copy-start.1 = (bf16[1,2048,1024]{2,1,0:T(8,128)(2,1)S(1)}, bf16[1,2048,1024]{2,1,0:T(8,128)(2,1)}, u32[]{:S(2)}) copy-start(bf16[1,2048,1024]{2,1,0:T(8,128)(2,1)} %param.12) | copy-start | bytes 12582916
  22.7 4.1 %copy-start = (bf16[1,1024,2048]{2,1,0:T(8,128)(2,1)S(1)}, bf16[1,1024,2048]{2,1,0:T(8,128)(2,1)}, u32[]{:S(2)}) copy-start(bf16[1,1024,2048]{2,1,0:T(8,128)(2,1)} %param.13) | copy-start | bytes 12582916
Sparse Core Ops, SparseCore 0:
  28.6 30.8 reduce-scatter.1
where the time goes:
time: 76 us; the launch traced here: 75.7 us
  waiting for transfers between devices  31.1 us (41%)
  blocking collectives  19.3 us (25%)
  between operations  13.5 us (18%)
  matrix products  7.61 us (10%)
  other arithmetic  3.18 us (4%)
  local copies, waits for them, and re-layouts  1.06 us (1%)
    reduce_scatter x1, waiting for transfers between devices, shards(): lax.psum_scatter(partial_value.reshape(sources, count, width), 'tp', scat...  31.1 us
    all_to_all x1, blocking collectives, shards(): lax.all_to_all(buffer, 'ep', split_axis=0, concat_axis=0, tiled=True)  10.7 us
    all_to_all x1, blocking collectives, shards(): lax.all_to_all(outputs, 'ep', split_axis=0, concat_axis=0, tiled=True)  8.59 us
    dot_general x1, matrix products, expert_rows(): gate = jnp.dot(rows, w_gate, preferred_element_type=jnp.float32)  3.18 us
    dot_general x1, matrix products, shards(): partial_value = jnp.dot(hidden, w_down, preferred_element_type=jnp.float32)  1.63 us
  transfers between devices with their start and end apart: 1, of which 1 were waited for; matrix products, arithmetic and copies ran while one was open for 0% of the time, Pallas kernels for 0%

commit v1 on v0

--- a/solution.py
+++ b/solution.py
@@ -1,7 +1,13 @@
+import functools
+
 import jax
 import jax.numpy as jnp
 from jax import lax
+from jax.experimental import pallas as pl
+from jax.experimental.pallas import tpu as pltpu
 from jax.sharding import PartitionSpec as P
+
+MESH = pl.DeviceIdType.MESH
 
 
 def expert_rows(rows, w_gate, w_up):
@@ -53,6 +59,206 @@
     return mixed.astype(jnp.bfloat16)
 
 
+def step_kernel(n_ep, n_z, cap, nk, tok_hbm, gain_ref, routes_ref, gw_ref, wg_hbm, wu_hbm, wd_hbm,
+                out_ref, tok, wg, wu, wd, sendbuf, recv, acc_g, acc_u, hid, pbuf, prbuf, obuf, fin,
+                tok_sem, wg_sem, wu_sem, wd_sem, d_send, d_recv, p_send, p_recv, f_send, f_recv):
+    me = lax.axis_index("ep")
+    t = lax.axis_index("tp")
+    z = t // 2
+    c = t % 2
+    other = 1 - c
+    partner = 2 * z + other
+    rows, width = tok.shape
+    ff = wg.shape[1]
+    kc = width // nk
+    pw = out_ref.shape[1]
+    slots_n = n_ep * cap
+
+    tok_copy = pltpu.make_async_copy(tok_hbm, tok, tok_sem)
+    tok_copy.start()
+
+    barrier = pltpu.get_barrier_semaphore()
+    pl.semaphore_signal(barrier, inc=1, device_id=(me, partner), device_id_type=MESH)
+    for dz in range(n_z):
+        for ds in range(n_ep):
+            if dz or ds:
+                dest = (lax.rem(me + ds, n_ep), 2 * lax.rem(z + dz, n_z) + c)
+                pl.semaphore_signal(barrier, inc=1, device_id=dest, device_id_type=MESH)
+
+    w_copies = []
+    for k in range(nk):
+        cut = pl.ds(k * kc, kc)
+        cg = pltpu.make_async_copy(wg_hbm.at[0, cut], wg.at[cut], wg_sem.at[k])
+        cu = pltpu.make_async_copy(wu_hbm.at[0, cut], wu.at[cut], wu_sem.at[k])
+        cg.start()
+        cu.start()
+        w_copies.append((cg, cu))
+    d_copy = pltpu.make_async_copy(wd_hbm.at[0], wd, wd_sem)
+    d_copy.start()
+
+    shape3 = (n_ep, cap, rows)
+    expert = lax.broadcasted_iota(jnp.int32, shape3, 0).reshape(slots_n, rows)
+    slot = lax.broadcasted_iota(jnp.int32, shape3, 1).reshape(slots_n, rows)
+    first = routes_ref[0:1, :] == expert
+    second = routes_ref[1:2, :] == expert
+    chosen = jnp.where(first | second, 1.0, 0.0)
+    before = jnp.where(
+        lax.broadcasted_iota(jnp.int32, (rows, rows), 0)
+        < lax.broadcasted_iota(jnp.int32, (rows, rows), 1), 1.0, 0.0)
+    rank = jnp.dot(chosen.astype(jnp.bfloat16), before.astype(jnp.bfloat16),
+                   preferred_element_type=jnp.float32)
+    table = jnp.where(rank == slot.astype(jnp.float32), chosen, 0.0)
+    weight = jnp.where(first, gw_ref[0:1, :], 0.0) + jnp.where(second, gw_ref[1:2, :], 0.0)
+    combine = (table * weight).T
+    table = table.astype(jnp.bfloat16)
+
+    tok_copy.wait()
+    values = tok[...].astype(jnp.float32)
+    scale = lax.rsqrt(jnp.mean(values * values, axis=-1, keepdims=True) + 1e-06)
+    for k in range(nk):
+        cut = slice(k * kc, (k + 1) * kc)
+        normed = (tok[:, cut].astype(jnp.float32) * scale * gain_ref[:, cut]).astype(jnp.bfloat16)
+        block = jnp.dot(table, normed, preferred_element_type=jnp.float32).astype(jnp.bfloat16)
+        sendbuf[k] = block.reshape(n_ep, cap, kc)
+    for k in range(nk):
+        recv[k, me] = sendbuf[k, me]
+
+    pl.semaphore_wait(barrier, n_z * n_ep)
+
+    dispatch = []
+    for k in range(nk):
+        per = []
+        for i in range(1, n_ep):
+            dest = lax.rem(me + i, n_ep)
+            copy = pltpu.make_async_remote_copy(
+                src_ref=sendbuf.at[k, dest], dst_ref=recv.at[k, me],
+                send_sem=d_send.at[k, i - 1], recv_sem=d_recv.at[k, i - 1],
+                device_id=(dest, t), device_id_type=MESH)
+            copy.start()
+            per.append(copy)
+        dispatch.append(per)
+
+    for k in range(nk):
+        w_copies[k][0].wait()
+        w_copies[k][1].wait()
+        for copy in dispatch[k]:
+            copy.wait_recv()
+        x = recv[k].reshape(slots_n, kc)
+        g = jnp.dot(x, wg[k * kc:(k + 1) * kc, :], preferred_element_type=jnp.float32)
+        u = jnp.dot(x, wu[k * kc:(k + 1) * kc, :], preferred_element_type=jnp.float32)
+        if k == 0:
+            acc_g[...] = g
+            acc_u[...] = u
+        elif k < nk - 1:
+            acc_g[...] += g
+            acc_u[...] += u
+        else:
+            g = acc_g[...] + g
+            u = acc_u[...] + u
+            hid[...] = (g / (1.0 + jnp.exp(-g)) * u).astype(jnp.bfloat16)
+
+    d_copy.wait()
+    order = sorted(range(n_z), key=lambda d: -min(d, n_z - d))
+    crossing = []
+    for j, dz in enumerate(order):
+        zz = lax.rem(z + dz, n_z)
+        cut = pl.ds(pl.multiple_of((2 * zz + other) * pw, 128), pw)
+        pbuf[j] = jnp.dot(hid[...], wd[:, cut], preferred_element_type=jnp.float32)
+        copy = pltpu.make_async_remote_copy(
+            src_ref=pbuf.at[j], dst_ref=prbuf.at[j], send_sem=p_send.at[j], recv_sem=p_recv.at[j],
+            device_id=(me, partner), device_id_type=MESH)
+        copy.start()
+        crossing.append(copy)
+    final = []
+    for j, dz in enumerate(order):
+        zz = lax.rem(z + dz, n_z)
+        cut = pl.ds(pl.multiple_of((2 * zz + c) * pw, 128), pw)
+        own = jnp.dot(hid[...], wd[:, cut], preferred_element_type=jnp.float32)
+        crossing[j].wait_recv()
+        block = (own + prbuf[j]).astype(jnp.bfloat16).reshape(n_ep, cap, pw)
+        obuf[j] = block
+        for ds in range(n_ep):
+            dest = lax.rem(me + ds, n_ep)
+            if dz or ds:
+                copy = pltpu.make_async_remote_copy(
+                    src_ref=obuf.at[j, dest], dst_ref=fin.at[z, me],
+                    send_sem=f_send.at[j, ds], recv_sem=f_recv.at[j, ds],
+                    device_id=(dest, 2 * zz + c), device_id_type=MESH)
+                copy.start()
+                final.append(copy)
+            else:
+                fin[z, me] = obuf[j, me]
+
+    for per in dispatch:
+        for copy in per:
+            copy.wait_send()
+    for copy in crossing:
+        copy.wait_send()
+    for copy in final:
+        copy.wait_recv()
+    total = fin[0].astype(jnp.float32)
+    for i in range(1, n_z):
+        total = total + fin[i].astype(jnp.float32)
+    mixed = jnp.dot(combine, total.reshape(slots_n, pw), precision=lax.Precision.HIGHEST,
+                    preferred_element_type=jnp.float32)
+    out_ref[...] = mixed.astype(jnp.bfloat16)
+    for copy in final:
+        copy.wait_send()
+
+
+def fused(tokens, norm_gain, routes, gate_weights, expert_gate, expert_up, expert_down):
+    rows, width = tokens.shape
+    n_ep = lax.axis_size("ep")
+    n_tp = lax.axis_size("tp")
+    n_z = n_tp // 2
+    pw = width // n_tp
+    cap = rows // 2
+    ff = expert_gate.shape[2]
+    slots_n = n_ep * cap
+    nk = 4
+    kc = width // nk
+    vmem = pl.BlockSpec(memory_space=pltpu.VMEM)
+    hbm = pl.BlockSpec(memory_space=pl.ANY)
+    bf, f32 = jnp.bfloat16, jnp.float32
+    dma = pltpu.SemaphoreType.DMA
+    return pl.pallas_call(
+        functools.partial(step_kernel, n_ep, n_z, cap, nk),
+        out_shape=jax.ShapeDtypeStruct((rows, pw), bf),
+        in_specs=[hbm, vmem, vmem, vmem, hbm, hbm, hbm],
+        out_specs=vmem,
+        scratch_shapes=[
+            pltpu.VMEM((rows, width), bf),
+            pltpu.VMEM((width, ff), bf),
+            pltpu.VMEM((width, ff), bf),
+            pltpu.VMEM((ff, width), bf),
+            pltpu.VMEM((nk, n_ep, cap, kc), bf),
+            pltpu.VMEM((nk, n_ep, cap, kc), bf),
+            pltpu.VMEM((slots_n, ff), f32),
+            pltpu.VMEM((slots_n, ff), f32),
+            pltpu.VMEM((slots_n, ff), bf),
+            pltpu.VMEM((n_z, slots_n, pw), f32),
+            pltpu.VMEM((n_z, slots_n, pw), f32),
+            pltpu.VMEM((n_z, n_ep, cap, pw), bf),
+            pltpu.VMEM((n_z, n_ep, cap, pw), bf),
+            dma, dma((nk,)), dma((nk,)), dma,
+            dma((nk, n_ep - 1)), dma((nk, n_ep - 1)),
+            dma((n_z,)), dma((n_z,)),
+            dma((n_z, n_ep)), dma((n_z, n_ep)),
+        ],
+        compiler_params=pltpu.CompilerParams(
+            collective_id=0, has_side_effects=True, vmem_limit_bytes=60 * 1024 * 1024),
+    )(tokens, norm_gain.reshape(1, width), routes.T, gate_weights.T, expert_gate, expert_up,
+      expert_down)
+
+
+def body(tokens, *rest):
+    rows, width = tokens.shape
+    n_tp = lax.axis_size("tp")
+    if n_tp % 2 == 0 and (width // n_tp) % 128 == 0 and rows % 32 == 0:
+        return fused(tokens, *rest)
+    return shards(tokens, *rest)
+
+
 def solution(mesh):
     placed = (
         P("ep", None),
@@ -64,5 +270,5 @@
         P("ep", "tp", None),
     )
     return jax.shard_map(
-        shards, mesh=mesh, in_specs=placed, out_specs=P("ep", "tp"), check_vma=False
-    )
+        body, mesh=mesh, in_specs=placed, out_specs=P("ep", "tp"), check_vma=False
+    )

time: 76 us -> 22.5 us (0.30)
  waiting for transfers between devices: 31.1 us -> 0 us
  Pallas kernels: 0 us -> 20.9 us
  blocking collectives: 19.3 us -> 0 us
  between operations: 13.5 us -> 0.01 us
  matrix products: 7.61 us -> 0 us
  other arithmetic: 3.18 us -> 0 us
    reduce_scatter x1 -> x0, waiting for transfers between devices: 31.1 us -> none  [shards(): lax.psum_scatter(partial_value.reshape(sources, count, width), 'tp', scat...]
    pallas_call x0 -> x1, Pallas kernels: none -> 20.9 us  [fused(): pl.pallas_call(functools.partial(step_kernel, n_ep, n_z, cap, nk), out_sh...]
    all_to_all x2 -> x0, blocking collectives: 19.3 us -> none  [the longest x1 10.7 us: shards(): lax.all_to_all(buffer, 'ep', split_axis=0, concat_axis=0, tiled=True)]
    dot_general x5 -> x0, matrix products: 7.61 us -> none  [the longest x1 3.18 us: expert_rows(): gate = jnp.dot(rows, w_gate, preferred_element_type=jnp.float32)]
    reduce_sum x3 -> x0, other arithmetic: 2.16 us -> none  [the longest x1 1.04 us: shards(): scale = lax.rsqrt(jnp.mean(values * values, axis=-1, keepdims=True) + 1e-06)]
    add x1 -> x0, other arithmetic: 0.85 us -> none  [shards(): place = picks * capacity + jnp.sum(ranks * chosen, axis=1)]
  transfers between devices with their start and end apart: 1 -> 0, of which waited for: 1 -> 0; matrix products, arithmetic and copies ran while one was open for 0% -> 0% of each run, Pallas kernels for 0% -> 0%
where the time goes in v1:
time: 22.5 us; the launch traced here: 22.3 us
  Pallas kernels  20.9 us (93%)
  local copies, waits for them, and re-layouts  1.32 us (6%)
    pallas_call x1, Pallas kernels, fused(): pl.pallas_call(functools.partial(step_kernel, n_ep, n_z, cap, nk), out_sh...  20.9 us
    unnamed x1, local copies, waits for them, and re-layouts  1.32 us

profile of v1, /device:TPU:0, one launch (start us, length us, event | category | flops | bytes accessed | tf_op | source)
XLA Modules:
  0.0 22.3 jit_solution(1634426579937419625)
XLA Ops:
  0.0 20.9 %shard_map.73 = bf16[32,256]{1,0:T(8,128)(2,1)} custom-call(bf16[32,2048]{1,0:T(8,128)(2,1)} %tok_hbm.1, f32[1,2048]{1,0:T(1,128)} %bitcast.3, s32[2,32]{1,0:T(2,128)} %bitcast.4, f32[2,32]{1,0:T(2,128)} %bitcast.5, bf16[1,2048,1024]{2,1,0:T(8,128)(2,1)} %wg_hbm.1, bf16[1,2048,1024]{2,1,0:T(8,128)(2,1)} %wu_hbm.1, bf16[1,1024,2048]{2,1,0:T(8,128)(2,1)} %wd_hbm.1), custom_call_target="tpu_custom_call" | custom-call | tf_op jit(solution)/shard_map/pallas_call | solution.py:224
  21.0 1.3 %copy.9 = bf16[32,256]{1,0:T(8,128)(2,1)} copy(bf16[32,256]{1,0:T(8,128)(2,1)} %shard_map.73) | data formatting | bytes 32768

commit v2 on v1

--- a/solution.py
+++ b/solution.py
@@ -59,9 +59,10 @@
     return mixed.astype(jnp.bfloat16)
 
 
-def step_kernel(n_ep, n_z, cap, nk, tok_hbm, gain_ref, routes_ref, gw_ref, wg_hbm, wu_hbm, wd_hbm,
-                out_ref, tok, wg, wu, wd, sendbuf, recv, acc_g, acc_u, hid, pbuf, prbuf, obuf, fin,
-                tok_sem, wg_sem, wu_sem, wd_sem, d_send, d_recv, p_send, p_recv, f_send, f_recv):
+def step_kernel(n_ep, n_z, cap, nk, tok_hbm, gain_hbm, routes_hbm, gw_hbm, wg_hbm, wu_hbm, wd_hbm,
+                out_ref, tok, gain_ref, routes_ref, gw_ref, wg, wu, wd, sendbuf, recv, acc_g, acc_u,
+                hid, pbuf, prbuf, obuf, fin, tok_sem, small_sem, wg_sem, wu_sem, wd_sem, d_send,
+                d_recv, p_send, p_recv, f_send, f_recv, line_sem):
     me = lax.axis_index("ep")
     t = lax.axis_index("tp")
     z = t // 2
@@ -69,21 +70,54 @@
     other = 1 - c
     partner = 2 * z + other
     rows, width = tok.shape
-    ff = wg.shape[1]
     kc = width // nk
     pw = out_ref.shape[1]
     slots_n = n_ep * cap
+    above = z < n_z - 1
+    below = z > 0
 
     tok_copy = pltpu.make_async_copy(tok_hbm, tok, tok_sem)
     tok_copy.start()
 
     barrier = pltpu.get_barrier_semaphore()
+    for i in range(1, n_ep):
+        pl.semaphore_signal(barrier, inc=1, device_id=(lax.rem(me + i, n_ep), t),
+                            device_id_type=MESH)
     pl.semaphore_signal(barrier, inc=1, device_id=(me, partner), device_id_type=MESH)
-    for dz in range(n_z):
-        for ds in range(n_ep):
-            if dz or ds:
-                dest = (lax.rem(me + ds, n_ep), 2 * lax.rem(z + dz, n_z) + c)
-                pl.semaphore_signal(barrier, inc=1, device_id=dest, device_id_type=MESH)
+
+    @pl.when(above)
+    def _():
+        pl.semaphore_signal(barrier, inc=1, device_id=(me, t + 2), device_id_type=MESH)
+
+    @pl.when(below)
+    def _():
+        pl.semaphore_signal(barrier, inc=1, device_id=(me, t - 2), device_id_type=MESH)
+
+    def line_signal(r):
+        @pl.when(above)
+        def _():
+            pl.semaphore_signal(line_sem.at[r, 0], inc=1, device_id=(me, t + 2),
+                                device_id_type=MESH)
+
+        @pl.when(below)
+        def _():
+            pl.semaphore_signal(line_sem.at[r, 1], inc=1, device_id=(me, t - 2),
+                                device_id_type=MESH)
+
+    def line_wait(r):
+        @pl.when(below)
+        def _():
+            pl.semaphore_wait(line_sem.at[r, 0], 1)
+
+        @pl.when(above)
+        def _():
+            pl.semaphore_wait(line_sem.at[r, 1], 1)
+
+    small = [pltpu.make_async_copy(routes_hbm, routes_ref, small_sem.at[0]),
+             pltpu.make_async_copy(gw_hbm, gw_ref, small_sem.at[1]),
+             pltpu.make_async_copy(gain_hbm, gain_ref, small_sem.at[2])]
+    for copy in small:
+        copy.start()
 
     w_copies = []
     for k in range(nk):
@@ -96,6 +130,8 @@
     d_copy = pltpu.make_async_copy(wd_hbm.at[0], wd, wd_sem)
     d_copy.start()
 
+    small[0].wait()
+    small[1].wait()
     shape3 = (n_ep, cap, rows)
     expert = lax.broadcasted_iota(jnp.int32, shape3, 0).reshape(slots_n, rows)
     slot = lax.broadcasted_iota(jnp.int32, shape3, 1).reshape(slots_n, rows)
@@ -113,6 +149,7 @@
     table = table.astype(jnp.bfloat16)
 
     tok_copy.wait()
+    small[2].wait()
     values = tok[...].astype(jnp.float32)
     scale = lax.rsqrt(jnp.mean(values * values, axis=-1, keepdims=True) + 1e-06)
     for k in range(nk):
@@ -123,7 +160,8 @@
     for k in range(nk):
         recv[k, me] = sendbuf[k, me]
 
-    pl.semaphore_wait(barrier, n_z * n_ep)
+    pl.semaphore_wait(barrier, n_ep + jnp.where(above, 1, 0) + jnp.where(below, 1, 0))
+    line_signal(0)
 
     dispatch = []
     for k in range(nk):
@@ -137,6 +175,9 @@
             copy.start()
             per.append(copy)
         dispatch.append(per)
+    for r in range(n_z - 2):
+        line_wait(r)
+        line_signal(r + 1)
 
     for k in range(nk):
         w_copies[k][0].wait()
@@ -158,10 +199,15 @@
             hid[...] = (g / (1.0 + jnp.exp(-g)) * u).astype(jnp.bfloat16)
 
     d_copy.wait()
-    order = sorted(range(n_z), key=lambda d: -min(d, n_z - d))
+    order = []
+    upper = 2 * z >= n_z
+    for j in range(n_z - 1):
+        down = n_z - 1 - j
+        order.append(jnp.where(upper, jnp.where(z <= j, j + 1, j),
+                               jnp.where(z >= down, down - 1, down)))
+    order.append(z)
     crossing = []
-    for j, dz in enumerate(order):
-        zz = lax.rem(z + dz, n_z)
+    for j, zz in enumerate(order):
         cut = pl.ds(pl.multiple_of((2 * zz + other) * pw, 128), pw)
         pbuf[j] = jnp.dot(hid[...], wd[:, cut], preferred_element_type=jnp.float32)
         copy = pltpu.make_async_remote_copy(
@@ -169,20 +215,22 @@
             device_id=(me, partner), device_id_type=MESH)
         copy.start()
         crossing.append(copy)
+    if n_z > 1:
+        line_wait(n_z - 2)
     final = []
-    for j, dz in enumerate(order):
-        zz = lax.rem(z + dz, n_z)
+    for j, zz in enumerate(order):
         cut = pl.ds(pl.multiple_of((2 * zz + c) * pw, 128), pw)
         own = jnp.dot(hid[...], wd[:, cut], preferred_element_type=jnp.float32)
         crossing[j].wait_recv()
-        block = (own + prbuf[j]).astype(jnp.bfloat16).reshape(n_ep, cap, pw)
-        obuf[j] = block
-        for ds in range(n_ep):
+        obuf[j] = (own + prbuf[j]).astype(jnp.bfloat16).reshape(n_ep, cap, pw)
+        mine = j == n_z - 1
+        gap = lax.rem(zz - z + n_z, n_z)
+        for ds in range(n_ep - 1, -1, -1):
             dest = lax.rem(me + ds, n_ep)
-            if dz or ds:
+            if ds or not mine:
                 copy = pltpu.make_async_remote_copy(
                     src_ref=obuf.at[j, dest], dst_ref=fin.at[z, me],
-                    send_sem=f_send.at[j, ds], recv_sem=f_recv.at[j, ds],
+                    send_sem=f_send.at[gap, ds], recv_sem=f_recv.at[gap, ds],
                     device_id=(dest, 2 * zz + c), device_id_type=MESH)
                 copy.start()
                 final.append(copy)
@@ -223,11 +271,14 @@
     dma = pltpu.SemaphoreType.DMA
     return pl.pallas_call(
         functools.partial(step_kernel, n_ep, n_z, cap, nk),
-        out_shape=jax.ShapeDtypeStruct((rows, pw), bf),
-        in_specs=[hbm, vmem, vmem, vmem, hbm, hbm, hbm],
+        out_shape=pltpu.VMEM((rows, pw), bf),
+        in_specs=[hbm] * 7,
         out_specs=vmem,
         scratch_shapes=[
             pltpu.VMEM((rows, width), bf),
+            pltpu.VMEM((1, width), f32),
+            pltpu.VMEM((2, rows), jnp.int32),
+            pltpu.VMEM((2, rows), f32),
             pltpu.VMEM((width, ff), bf),
             pltpu.VMEM((width, ff), bf),
             pltpu.VMEM((ff, width), bf),
@@ -240,10 +291,11 @@
             pltpu.VMEM((n_z, slots_n, pw), f32),
             pltpu.VMEM((n_z, n_ep, cap, pw), bf),
             pltpu.VMEM((n_z, n_ep, cap, pw), bf),
-            dma, dma((nk,)), dma((nk,)), dma,
+            dma, dma((3,)), dma((nk,)), dma((nk,)), dma,
             dma((nk, n_ep - 1)), dma((nk, n_ep - 1)),
             dma((n_z,)), dma((n_z,)),
             dma((n_z, n_ep)), dma((n_z, n_ep)),
+            pltpu.SemaphoreType.REGULAR((max(n_z - 1, 1), 2)),
         ],
         compiler_params=pltpu.CompilerParams(
             collective_id=0, has_side_effects=True, vmem_limit_bytes=60 * 1024 * 1024),

time: 22.5 us -> 19.9 us (0.88)
  Pallas kernels: 20.9 us -> 19.2 us
  local copies, waits for them, and re-layouts: 1.32 us -> 0.61 us
    pallas_call x1, Pallas kernels: 20.9 us -> 19.2 us  [fused(): pl.pallas_call(functools.partial(step_kernel, n_ep, n_z, cap, nk), out_sh...]
    unnamed x1, local copies, waits for them, and re-layouts: 1.32 us -> 0.61 us
where the time goes in v2:
time: 19.9 us; the launch traced here: 19.8 us
  Pallas kernels  19.2 us (96%)
  local copies, waits for them, and re-layouts  0.61 us (3%)
    pallas_call x1, Pallas kernels, fused(): pl.pallas_call(functools.partial(step_kernel, n_ep, n_z, cap, nk), out_sh...  19.2 us
    unnamed x1, local copies, waits for them, and re-layouts  0.61 us

profile of v2, /device:TPU:0, one launch (start us, length us, event | category | flops | bytes accessed | tf_op | source)
XLA Modules:
  0.0 19.8 jit_solution(4271062017909017120)
XLA Ops:
  0.0 19.2 %shard_map.73 = bf16[32,256]{1,0:T(8,128)(2,1)S(1)} custom-call(bf16[32,2048]{1,0:T(8,128)(2,1)} %tok_hbm.1, f32[1,2048]{1,0:T(1,128)} %bitcast.3, s32[2,32]{1,0:T(2,128)} %bitcast.4, f32[2,32]{1,0:T(2,128)} %bitcast.5, bf16[1,2048,1024]{2,1,0:T(8,128)(2,1)} %wg_hbm.1, bf16[1,2048,1024]{2,1,0:T(8,128)(2,1)} %wu_hbm.1, bf16[1,1024,2048]{2,1,0:T(8,128)(2,1)} %wd_hbm.1), custom_call_target="tpu_custom_call" | custom-call | tf_op jit(solution)/shard_map/pallas_call | solution.py:272
  19.2 0.6 %copy.9 = bf16[32,256]{1,0:T(8,128)(2,1)} copy(bf16[32,256]{1,0:T(8,128)(2,1)S(1)} %shard_map.73) | data formatting | bytes 32768

commit v3 on v2

--- a/solution.py
+++ b/solution.py
@@ -161,7 +161,6 @@
         recv[k, me] = sendbuf[k, me]
 
     pl.semaphore_wait(barrier, n_ep + jnp.where(above, 1, 0) + jnp.where(below, 1, 0))
-    line_signal(0)
 
     dispatch = []
     for k in range(nk):
@@ -175,6 +174,7 @@
             copy.start()
             per.append(copy)
         dispatch.append(per)
+    line_signal(0)
     for r in range(n_z - 2):
         line_wait(r)
         line_signal(r + 1)
@@ -187,7 +187,9 @@
         x = recv[k].reshape(slots_n, kc)
         g = jnp.dot(x, wg[k * kc:(k + 1) * kc, :], preferred_element_type=jnp.float32)
         u = jnp.dot(x, wu[k * kc:(k + 1) * kc, :], preferred_element_type=jnp.float32)
-        if k == 0:
+        if nk == 1:
+            hid[...] = (g / (1.0 + jnp.exp(-g)) * u).astype(jnp.bfloat16)
+        elif k == 0:
             acc_g[...] = g
             acc_u[...] = u
         elif k < nk - 1:
@@ -263,7 +265,7 @@
     cap = rows // 2
     ff = expert_gate.shape[2]
     slots_n = n_ep * cap
-    nk = 4
+    nk = 2
     kc = width // nk
     vmem = pl.BlockSpec(memory_space=pltpu.VMEM)
     hbm = pl.BlockSpec(memory_space=pl.ANY)

time: 19.9 us -> 19.4 us (0.975)
  Pallas kernels: 19.2 us -> 18.7 us
    pallas_call x1, Pallas kernels: 19.2 us -> 18.7 us  [fused(): pl.pallas_call(functools.partial(step_kernel, n_ep, n_z, cap, nk), out_sh...]
where the time goes in v3:
time: 19.4 us; the launch traced here: 19.3 us
  Pallas kernels  18.7 us (96%)
  local copies, waits for them, and re-layouts  0.61 us (3%)
    pallas_call x1, Pallas kernels, fused(): pl.pallas_call(functools.partial(step_kernel, n_ep, n_z, cap, nk), out_sh...  18.7 us
    unnamed x1, local copies, waits for them, and re-layouts  0.61 us

profile of v3, /device:TPU:0, one launch (start us, length us, event | category | flops | bytes accessed | tf_op | source)
XLA Modules:
  0.0 19.3 jit_solution(16906595601882203243)
XLA Ops:
  0.0 18.7 %shard_map.73 = bf16[32,256]{1,0:T(8,128)(2,1)S(1)} custom-call(bf16[32,2048]{1,0:T(8,128)(2,1)} %tok_hbm.1, f32[1,2048]{1,0:T(1,128)} %bitcast.3, s32[2,32]{1,0:T(2,128)} %bitcast.4, f32[2,32]{1,0:T(2,128)} %bitcast.5, bf16[1,2048,1024]{2,1,0:T(8,128)(2,1)} %wg_hbm.1, bf16[1,2048,1024]{2,1,0:T(8,128)(2,1)} %wu_hbm.1, bf16[1,1024,2048]{2,1,0:T(8,128)(2,1)} %wd_hbm.1), custom_call_target="tpu_custom_call" | custom-call | tf_op jit(solution)/shard_map/pallas_call | solution.py:274
  18.7 0.6 %copy.9 = bf16[32,256]{1,0:T(8,128)(2,1)} copy(bf16[32,256]{1,0:T(8,128)(2,1)S(1)} %shard_map.73) | data formatting | bytes 32768
